TPU v7x, 32 devices: a whole 2x2x4 slice. The times are simulated.
32 devices in a mesh: ep: 16 (over z, x, core), tp: 2 (over y).
Axes of the slice: x: 2, y: 2, z: 4, core: 2. Of those that a mesh axis runs over, the one named last changes fastest.
Arguments:
- hidden_in: bfloat16 [320, 2048], P('ep', 'tp'), may hold values from -32 to 32
- attn_gain: float32 [2048], replicated, may hold values from 0.1 to 1.9
- w_query: bfloat16 [256, 2048], P('tp'), may hold values from -0.125 to 0.125
- w_key: bfloat16 [256, 2048], P('tp'), may hold values from -0.125 to 0.125
- w_value: bfloat16 [256, 2048], P('tp'), may hold values from -0.125 to 0.125
- break_bias: float32 [4], P('tp'), may hold values from -9 to -3
- key_cache: bfloat16 [320, 256, 512], P('ep', 'tp'), may hold values from -6 to 6
- value_cache: bfloat16 [320, 256, 512], P('ep', 'tp'), may hold values from -8 to 8
- lengths: int32 [320], P('ep'), may hold values from 32 to 512
- w_out: bfloat16 [256, 2048], P('tp'), may hold values from -0.375 to 0.375
- ffn_gain: float32 [2048], replicated, may hold values from 0.1 to 1.9
- route_ids: int32 [320, 6], P('ep'), may hold values from 0 to 15, all different within a row; in each aligned block of 20 rows (0 to 19, 20 to 39, ...) at most 15 rows name the same one
- route_scores: float32 [320, 6], P('ep'), may hold values from 0.05 to 1
- expert_gate: bfloat16 [16, 2048, 512], P('ep', None, 'tp'), may hold values from -0.125 to 0.125
- expert_up: bfloat16 [16, 2048, 512], P('ep', None, 'tp'), may hold values from -0.125 to 0.125
- expert_down: bfloat16 [16, 512, 2048], P('ep', 'tp'), may hold values from -0.25 to 0.25
Outputs:
- hidden_out: bfloat16 [320, 2048], P('ep', 'tp')
- new_keys: bfloat16 [320, 256], P('ep', 'tp')
- new_values: bfloat16 [320, 256], P('ep', 'tp')
Inputs may be any that keep to these rules, and one draw needn't show every extreme that they name: `route_ids`: each row names 6 distinct experts. Within each aligned block of 20 rows (the rows of one device) no expert is named more than 15 times, a bound that some block reaches.
All inputs are finite; a program needn't handle non-finite values.
Results may differ from a plain program's by a relative error of at most 0.0055.
Values may be sent and summed in bfloat16 or wider, within the bound.
A program may use at most 64 MiB of HBM per device.

v0:
```python
import jax
import jax.numpy as jnp
from jax import lax
from jax.sharding import PartitionSpec as P

HEAD_DIM = 64


norm_eps = 1e-06


def rms_norm(row_values, norm_gain):
    values = row_values.astype(jnp.float32)
    inverse_rms = lax.rsqrt(jnp.mean(values * values, axis=-1, keepdims=True) + norm_eps)
    return (values * inverse_rms * norm_gain).astype(jnp.bfloat16)


def project_rows(normed, weight):
    return lax.dot_general(
        normed, weight, (((1,), (1,)), ((), ())), preferred_element_type=jnp.float32
    ).astype(jnp.bfloat16)


def stick_breaking(queries, key_block, value_block, lengths, break_bias):
    head_count = break_bias.shape[0]
    q_heads = queries.reshape(queries.shape[0], head_count, HEAD_DIM)
    k_heads = key_block.reshape(key_block.shape[0], head_count, HEAD_DIM, key_block.shape[2])
    v_heads = value_block.reshape(value_block.shape[0], head_count, HEAD_DIM, value_block.shape[2])
    logit = jnp.einsum("shd,shdl->shl", q_heads, k_heads, preferred_element_type=jnp.float32)
    logit = logit * HEAD_DIM ** (-0.5) + break_bias[None, :, None]
    position = jnp.arange(key_block.shape[2], dtype=jnp.int32)
    visible = (position[None, :] < lengths[:, None])[:, None, :]
    log_keep = jnp.where(visible, jax.nn.log_sigmoid(-logit), 0.0)
    later_sum = lax.cumsum(log_keep, axis=2, reverse=True) - log_keep
    stick = jnp.where(visible, jnp.exp(jax.nn.log_sigmoid(logit) + later_sum), 0.0).astype(
        jnp.bfloat16
    )
    attended = jnp.einsum("shl,shdl->shd", stick, v_heads, preferred_element_type=jnp.float32)
    return attended.reshape(queries.shape[0], -1).astype(jnp.bfloat16)


def shards(
    hidden_in,
    attn_gain,
    w_query,
    w_key,
    w_value,
    break_bias,
    key_cache,
    value_cache,
    lengths,
    w_out,
    ffn_gain,
    route_ids,
    route_scores,
    expert_gate,
    expert_up,
    expert_down,
):
    gathered = lax.all_gather(hidden_in, "tp", axis=1, tiled=True)
    full_width = gathered.shape[1]
    slice_width = hidden_in.shape[1]
    offset = lax.axis_index("tp") * slice_width
    normed_attn = rms_norm(gathered, attn_gain)
    queries = project_rows(normed_attn, w_query)
    new_keys = project_rows(normed_attn, w_key)
    new_values = project_rows(normed_attn, w_value)
    attended = stick_breaking(queries, key_cache, value_cache, lengths, break_bias)
    partial_out = jnp.dot(attended, w_out, preferred_element_type=jnp.float32)
    mixer_part = lax.psum_scatter(partial_out, "tp", scatter_dimension=1, tiled=True)
    residual = (hidden_in.astype(jnp.float32) + mixer_part).astype(jnp.bfloat16)
    resid_values = residual.astype(jnp.float32)
    square_total = lax.psum(jnp.sum(resid_values * resid_values, axis=1), "tp")
    inverse_rms = lax.rsqrt(square_total / full_width + norm_eps)
    gain_part = lax.dynamic_slice_in_dim(ffn_gain, offset, slice_width)
    normed_part = (resid_values * inverse_rms[:, None] * gain_part[None, :]).astype(jnp.bfloat16)
    seq_count = hidden_in.shape[0]
    route_count = route_ids.shape[1]
    local_experts = expert_gate.shape[0]
    experts = local_experts * lax.axis_size("ep")
    capacity = min(seq_count, max(2, 2 * seq_count * route_count // experts))
    flat_ids = route_ids.reshape(-1)
    expert_iota = jnp.arange(experts, dtype=jnp.int32)
    onehot = (flat_ids[:, None] == expert_iota[None, :]).astype(jnp.int32)
    earlier = jnp.cumsum(onehot, axis=0) - onehot
    slot_index = flat_ids * capacity + jnp.sum(earlier * onehot, axis=1)
    slot_iota = jnp.arange(experts * capacity, dtype=jnp.int32)
    placement = (slot_index[:, None] == slot_iota[None, :]).astype(jnp.bfloat16)
    repeated = jnp.repeat(normed_part, route_count, axis=0)
    outgoing = jnp.einsum("ke,kd->ed", placement, repeated, preferred_element_type=jnp.float32)
    full_rows = lax.all_gather(
        lax.all_to_all(
            outgoing.astype(jnp.bfloat16).reshape(experts, capacity, normed_part.shape[1]),
            "ep",
            split_axis=0,
            concat_axis=0,
            tiled=True,
        ),
        "tp",
        axis=2,
        tiled=True,
    )
    senders = full_rows.shape[0] // local_experts
    grouped = full_rows.reshape(senders, local_experts, full_rows.shape[1], full_rows.shape[2])
    gate_act = jnp.einsum(
        "secd,edf->secf", grouped, expert_gate, preferred_element_type=jnp.float32
    )
    up_act = jnp.einsum("secd,edf->secf", grouped, expert_up, preferred_element_type=jnp.float32)
    hidden = (jax.nn.silu(gate_act) * up_act).astype(jnp.bfloat16)
    partial_value = jnp.einsum(
        "secf,efd->secd", hidden, expert_down, preferred_element_type=jnp.float32
    )
    partial_value = partial_value.astype(jnp.bfloat16)
    summed = lax.psum_scatter(
        partial_value.astype(jnp.float32).astype(jnp.bfloat16),
        "tp",
        scatter_dimension=3,
        tiled=True,
    )
    summed = summed.reshape(senders * local_experts, summed.shape[2], summed.shape[3])
    returned = lax.all_to_all(summed, "ep", split_axis=0, concat_axis=0, tiled=True)
    flat_back = returned.reshape(experts * capacity, returned.shape[2])
    picked = jnp.take(flat_back, slot_index, axis=0)
    picked = picked.astype(jnp.float32).reshape(seq_count, route_count, slice_width)
    route_weight = route_scores / jnp.sum(route_scores, axis=1, keepdims=True)
    expert_mix = jnp.sum(picked * route_weight[:, :, None], axis=1)
    hidden_out = (residual.astype(jnp.float32) + expert_mix).astype(jnp.bfloat16)
    return (hidden_out, new_keys, new_values)


def solution(mesh):
    return jax.shard_map(
        shards,
        mesh=mesh,
        in_specs=(
            P("ep", "tp"),
            P(),
            P("tp", None),
            P("tp", None),
            P("tp", None),
            P("tp"),
            P("ep", "tp", None),
            P("ep", "tp", None),
            P("ep"),
            P("tp", None),
            P(),
            P("ep", None),
            P("ep", None),
            P("ep", None, "tp"),
            P("ep", None, "tp"),
            P("ep", "tp", None),
        ),
        out_specs=(P("ep", "tp"), P("ep", "tp"), P("ep", "tp")),
        check_vma=False,
    )
```

profile of v0, /device:TPU:0, one launch (start us, length us, event | category | flops | bytes accessed | tf_op | source)
XLA Modules:
  0.0 144.0 jit_solution(9065805730597150897)
XLA Ops:
  7.2 0.0 copy-start
  7.2 0.0 copy-start.11
  7.2 0.0 reduce-scatter.3.cloned.1.call-start
  7.2 0.9 iota_compare_fusion.3
  8.1 6.0 %all_gather.6 = bf16[20,2048]{1,0:T(8,128)(2,1)S(1)} all-gather(bf16[20,1024]{1,0:T(8,128)(2,1)} %param.16), channel_id=1, replica_groups=mesh['ep'=16,'tp'=2] {'tp'}, dimensions={1}, use_global_device_ids=true | all-gather | bytes 122880 | tf_op jit(solution)/shard_map/all_gather | solution.py:60
  14.1 0.1 fusion.14
  14.3 0.5 copy-done.9
  14.8 1.3 convolution_convert_fusion.4
  16.1 0.1 reshape.172
  16.2 0.0 copy-done
  16.2 0.5 fusion.38
  16.7 0.0 copy-done.6
  16.7 0.0 copy-done.11
  16.7 0.0 copy-start.3
  16.7 0.3 fusion.26
  17.0 0.1 reshape.144
  17.1 10.0 %reduce-window.6 = f32[20,2,4,128]{3,0,1,2:T(8,128)S(1)} reduce-window(f32[20,2,4,128]{3,0,1,2:T(8,128)S(1)} %copy.32, f32[]{:T(128)} %constant.21.clone.1), window={size=1x1x1x128 pad=0_0x0_0x0_0x0_127}, to_apply=%region_1.2 | reduce-window | flops 2600960 | bytes 163844 | tf_op jit(solution)/shard_map/reduce-window
  27.1 0.1 copy.33
  27.3 0.1 broadcast_add_fusion
  27.4 0.1 reduce_window_sum.26
  27.5 1.3 fusion.32
  28.8 2.5 %fusion.28 = f32[20,2,1,64]{3,2,1,0:T(1,128)S(1)} fusion(bf16[20,2,64,512]{3,2,1,0:T(8,128)(2,1)} %bitcast.85, bf16[20,2,512,1]{2,1,0,3:T(2,128)(2,1)S(1)} %fusion.32), kind=kOutput, calls=%fused_computation.45 | convolution fusion | flops 2621440 | bytes 2672640 | tf_op jit(solution)/shard_map/shl,shdl->shd/dot_general | solution.py:38
  31.3 0.1 convert_element_type.74
  31.4 0.0 copy-done.3
  31.4 0.9 fusion.39
  32.3 0.0 reduce-scatter.3.cloned.1.call-update
  32.3 0.0 reduce-scatter.5.cloned.1.call-start
  32.3 0.8 copy.36
  33.1 0.1 reshape.147
  33.2 0.1 fusion.31
  33.3 0.2 reduce_window_sum.27
  33.5 0.7 dynamic_slice.3
  34.2 0.2 select_reduce_fusion
  34.3 10.8 %reduce-scatter.3.cloned.1.call-done = f32[20,1024]{1,0:T(8,128)} async-done(((f32[20,2048]{1,0:T(8,128)}), f32[20,1024]{1,0:T(8,128)}) %reduce-scatter.3.cloned.1.call-update) | async-done | bytes 81936 | tf_op jit(solution)/shard_map/reduce_scatter | solution.py:70
  45.2 0.0 copy-done.5
  45.2 1.0 fusion.18
  46.2 4.9 %psum.7 = f32[20]{0:T(128)S(1)} all-reduce(f32[20]{0:T(128)S(1)} %get-tuple-element.3), channel_id=1, replica_groups=mesh['ep'=16,'tp'=2] {'tp'}, use_global_device_ids=true, to_apply=%region_7.8 | all-reduce | flops 20 | bytes 160 | tf_op jit(solution)/shard_map/psum | solution.py:73
  51.1 0.1 fusion.20
  51.3 0.1 reshape.148
  51.4 1.2 convolution_convert_fusion.1
  52.5 1.2 reshape.149
  53.7 0.0 copy-start.2
  53.7 19.8 %all_to_all.10 = bf16[16,15,1024]{2,1,0:T(8,128)(2,1)S(1)} all-to-all(bf16[16,15,1024]{2,1,0:T(8,128)(2,1)S(1)} %reshape.149), channel_id=1, replica_groups=mesh['ep'=16,'tp'=2] {'ep'}, dimensions={0} | all-to-all | bytes 983040 | tf_op jit(solution)/shard_map/all_to_all | solution.py:92
  73.6 0.3 copy.38
  73.9 13.9 %all_gather.7 = bf16[16,15,2048]{2,0,1:T(8,128)(2,1)S(1)} all-gather(bf16[16,15,1024]{2,0,1:T(8,128)(2,1)S(1)} %copy.38), channel_id=1, replica_groups=mesh['ep'=16,'tp'=2] {'tp'}, dimensions={2}, use_global_device_ids=true | all-gather | bytes 1474560 | tf_op jit(solution)/shard_map/all_gather | solution.py:91
  87.8 1.0 copy-done.1
  88.8 0.4 convolution_bitcast_fusion.1
  89.2 0.0 copy-start.8
  89.2 4.0 %fusion = bf16[16,1,15,2048]{3,0,2,1:T(8,128)(2,1)} fusion(bf16[1,256,2048]{2,1,0:T(8,128)(2,1)} %param.31, bf16[16,15,2048]{2,0,1:T(8,128)(2,1)} %copy-done.1, bf16[1,2048,256]{2,1,0:T(8,128)(2,1)} %param.30, f32[16,1,15,256]{3,0,2,1:T(8,128)S(1)} %convolution_bitcast_fusion.1), kind=kOutput, calls=%fused_computation.2 | convolution fusion | flops 504176640 | bytes 4308992 | tf_op jit(solution)/shard_map/secf,efd->secd/dot_general | solution.py:110
  93.3 0.0 reduce-scatter.5.cloned.1.call-update
  93.3 0.1 mul.111
  93.4 18.5 %reduce-scatter.5.cloned.1.call-done = bf16[16,1,15,1024]{3,0,2,1:T(8,128)(2,1)} async-done(((bf16[16,1,15,2048]{3,0,2,1:T(8,128)(2,1)}), bf16[16,1,15,1024]{3,0,2,1:T(8,128)(2,1)}) %reduce-scatter.5.cloned.1.call-update) | async-done | bytes 491536 | tf_op jit(solution)/shard_map/reduce_scatter | solution.py:114
  111.9 2.1 %copy.39 = bf16[16,15,1024]{2,1,0:T(8,128)(2,1)} copy(bf16[16,15,1024]{2,0,1:T(8,128)(2,1)} %bitcast.82) | data formatting | bytes 983040 | tf_op jit(solution)/shard_map/reshape | solution.py:120
  114.0 5.7 %all-to-all-start.1 = ((bf16[16,15,1024]{2,1,0:T(8,128)(2,1)}), bf16[16,15,1024]{2,1,0:T(8,128)(2,1)}, u32[]{:S(2)}, u32[]{:S(2)}) async-start(bf16[16,15,1024]{2,1,0:T(8,128)(2,1)} %copy.39), calls=%async_computation.3 | async-start | bytes 1048576 | tf_op jit(solution)/shard_map/all_to_all | solution.py:121
  119.7 0.1 reduce_sum.51
  119.8 0.1 copy.40
  119.9 0.9 convolution_convert_fusion.3
  120.8 1.9 %convolution_convert_fusion.2 = bf16[20,128]{1,0:T(8,128)(2,1)} fusion(bf16[128,2048]{1,0:T(8,128)(2,1)} %param.20, bf16[20,2048]{1,0:T(8,128)(2,1)S(1)} %all_gather.6, f32[2048]{0:T(1024)S(1)} %copy-done.7, f32[20]{0:T(128)S(1)} %copy-done.10), kind=kOutput, calls=%fused_computation.9 | convolution fusion | flops 10652160 | bytes 619600 | tf_op jit(solution)/shard_map/dot_general | solution.py:19
  122.8 11.2 %all-to-all-done.1 = bf16[16,15,1024]{2,1,0:T(8,128)(2,1)} async-done(((bf16[16,15,1024]{2,1,0:T(8,128)(2,1)}), bf16[16,15,1024]{2,1,0:T(8,128)(2,1)}, u32[]{:S(2)}, u32[]{:S(2)}) %all-to-all-start.1) | async-done | bytes 491552 | tf_op jit(solution)/shard_map/all_to_all | solution.py:121
  134.0 1.2 reshape.155
  135.2 0.8 gather_fusion
  136.1 0.1 gather.7
  136.1 0.4 multiply_reduce_fusion
  136.5 0.6 fusion.21
  (28 shorter events, 0.3 us)
Async XLA Ops:
  7.2 9.1 %copy-start = (bf16[20,128,512]{2,1,0:T(8,128)(2,1)S(1)}, bf16[20,128,512]{2,1,0:T(8,128)(2,1)}, u32[]{:S(2)}) copy-start(bf16[20,128,512]{2,1,0:T(8,128)(2,1)} %param.22) | copy-start | bytes 7864324
  7.2 9.5 %copy-start.11 = (f32[2]{0:T(128)S(1)}, f32[2]{0:T(128)}, u32[]{:S(2)}) copy-start(f32[2]{0:T(128)} %param.21) | copy-start | bytes 28
  7.2 38.0 %reduce-scatter.3.cloned.1.call-start = ((), (), s32[]{:S(2)}) async-start(), calls=%async_computation.4 | async-start | bytes 294912 | tf_op jit(solution)/shard_map/reduce_scatter | solution.py:70
  8.1 8.6 %copy-start.6 = (pred[20,512]{1,0:T(8,128)(4,1)}, pred[20,512]{1,0:T(8,128)(4,1)S(1)}, u32[]{:S(2)}) copy-start(pred[20,512]{1,0:T(8,128)(4,1)S(1)} %iota_compare_fusion.3) | copy-start | bytes 30724
  14.3 0.5 copy-start.9
  16.7 14.7 %copy-start.3 = (bf16[128,2048]{1,0:T(8,128)(2,1)S(1)}, bf16[128,2048]{1,0:T(8,128)(2,1)}, u32[]{:S(2)}) copy-start(bf16[128,2048]{1,0:T(8,128)(2,1)} %param.25) | copy-start | bytes 1572868
  27.1 18.1 %copy-start.5 = (bf16[20,1024]{1,0:T(8,128)(2,1)S(1)}, bf16[20,1024]{1,0:T(8,128)(2,1)}, u32[]{:S(2)}) copy-start(bf16[20,1024]{1,0:T(8,128)(2,1)} %param.16) | copy-start | bytes 122884
  32.3 79.6 %reduce-scatter.5.cloned.1.call-start = ((), (), s32[]{:S(2)}) async-start(), calls=%async_computation.5 | async-start | bytes 1474560 | tf_op jit(solution)/shard_map/reduce_scatter | solution.py:114
  53.7 35.1 %copy-start.2 = (bf16[1,2048,256]{2,1,0:T(8,128)(2,1)S(1)}, bf16[1,2048,256]{2,1,0:T(8,128)(2,1)}, u32[]{:S(2)}) copy-start(bf16[1,2048,256]{2,1,0:T(8,128)(2,1)} %param.29) | copy-start | bytes 3145732
  87.8 1.0 copy-start.1
  89.2 4.1 %copy-start.8 = (f32[20,6]{0,1:T(8,128)S(1)}, f32[20,6]{0,1:T(8,128)}, u32[]{:S(2)}) copy-start(f32[20,6]{0,1:T(8,128)} %param.28) | copy-start | bytes 1444
  93.2 26.7 %copy-start.4 = (bf16[128,2048]{1,0:T(8,128)(2,1)S(1)}, bf16[128,2048]{1,0:T(8,128)(2,1)}, u32[]{:S(2)}) copy-start(bf16[128,2048]{1,0:T(8,128)(2,1)} %param.19) | copy-start | bytes 1572868
  93.2 26.7 %copy-start.7 = (f32[2048]{0:T(1024)S(1)}, f32[2048]{0:T(1024)}, u32[]{:S(2)}) copy-start(f32[2048]{0:T(1024)} %param.17) | copy-start | bytes 24580
  93.3 26.7 %copy-start.10 = (f32[20]{0:T(128)S(1)}, f32[20]{0:T(128)}, u32[]{:S(2)}) copy-start(f32[20]{0:T(128)} %copy-done.9) | copy-start | bytes 244
  114.0 20.0 %all-to-all-start.1 = ((bf16[16,15,1024]{2,1,0:T(8,128)(2,1)}), bf16[16,15,1024]{2,1,0:T(8,128)(2,1)}, u32[]{:S(2)}, u32[]{:S(2)}) async-start(bf16[16,15,1024]{2,1,0:T(8,128)(2,1)} %copy.39), calls=%async_computation.3 | async-start | bytes 1048576 | tf_op jit(solution)/shard_map/all_to_all | solution.py:121
Sparse Core Ops, SparseCore 0:
  32.4 12.7 reduce-scatter.2
  93.4 18.4 reduce-scatter.4
where the time goes:
time: 145 us; the launch traced here: 144 us
  blocking collectives  44.7 us (31%)
  waiting for transfers between devices  40.6 us (28%)
  other arithmetic  15.3 us (11%)
  between operations  14.3 us (10%)
  matrix products  13.6 us (9%)
  local copies, waits for them, and re-layouts  9.72 us (7%)
  starting transfers between devices  5.75 us (4%)
    all_to_all x1, blocking collectives, shards(): lax.all_to_all(outgoing.astype(jnp.bfloat16).reshape(experts, capacity, n...  19.8 us
    reduce_scatter x1, waiting for transfers between devices, shards(): lax.psum_scatter(partial_value.astype(jnp.float32).astype(jnp.bfloat16),...  18.5 us
    all_gather x1, blocking collectives, shards(): lax.all_gather(lax.all_to_all(outgoing.astype(jnp.bfloat16).reshape(exper...  13.9 us
    all_to_all x1, waiting for transfers between devices, shards(): lax.all_to_all(summed, 'ep', split_axis=0, concat_axis=0, tiled=True)  11.2 us
    reduce_scatter x1, waiting for transfers between devices, shards(): lax.psum_scatter(partial_out, 'tp', scatter_dimension=1, tiled=True)  10.8 us
    another operation x2, other arithmetic  10 us
    all_gather x1, blocking collectives, shards(): gathered = lax.all_gather(hidden_in, 'tp', axis=1, tiled=True)  5.99 us
    all_to_all x1, starting transfers between devices, shards(): lax.all_to_all(summed, 'ep', split_axis=0, concat_axis=0, tiled=True)  5.67 us
  transfers between devices with their start and end apart: 3, of which 3 were waited for; matrix products, arithmetic and copies ran while one was open for 4% of the time, Pallas kernels for 0%

commit v1 on v0

--- a/solution.py
+++ b/solution.py
@@ -1,6 +1,10 @@
+import functools
+
 import jax
 import jax.numpy as jnp
 from jax import lax
+from jax.experimental import pallas as pl
+from jax.experimental.pallas import tpu as pltpu
 from jax.sharding import PartitionSpec as P
 
 HEAD_DIM = 64
@@ -19,6 +23,20 @@
     return lax.dot_general(
         normed, weight, (((1,), (1,)), ((), ())), preferred_element_type=jnp.float32
     ).astype(jnp.bfloat16)
+
+
+def sum_later(values):
+    span = values.shape[-1]
+    flat = values.reshape(-1, span)
+    row = lax.broadcasted_iota(jnp.int32, (span, span), 0)
+    col = lax.broadcasted_iota(jnp.int32, (span, span), 1)
+    later = (row > col).astype(jnp.bfloat16)
+    total, rest = 0.0, flat
+    for _ in range(3):
+        term = rest.astype(jnp.bfloat16)
+        rest = rest - term.astype(jnp.float32)
+        total = total + jnp.dot(term, later, preferred_element_type=jnp.float32)
+    return total.reshape(values.shape)
 
 
 def stick_breaking(queries, key_block, value_block, lengths, break_bias):
@@ -31,7 +49,7 @@
     position = jnp.arange(key_block.shape[2], dtype=jnp.int32)
     visible = (position[None, :] < lengths[:, None])[:, None, :]
     log_keep = jnp.where(visible, jax.nn.log_sigmoid(-logit), 0.0)
-    later_sum = lax.cumsum(log_keep, axis=2, reverse=True) - log_keep
+    later_sum = sum_later(log_keep)
     stick = jnp.where(visible, jnp.exp(jax.nn.log_sigmoid(logit) + later_sum), 0.0).astype(
         jnp.bfloat16
     )
@@ -128,9 +146,339 @@
     return (hidden_out, new_keys, new_values)
 
 
+def experts_kernel(
+    sizes,
+    part_ref,
+    hid_ref,
+    gain_ref,
+    wts_ref,
+    gate_hbm,
+    up_hbm,
+    down_hbm,
+    out_ref,
+    gate_w,
+    up_w,
+    down_w,
+    part_in,
+    resid,
+    rows,
+    own,
+    for_sib,
+    from_sib,
+    stage_a,
+    recv_a,
+    stage_b,
+    recv_b,
+    stage_c,
+    recv_c,
+    stage_d,
+    recv_d,
+    load_sem,
+    pair_send,
+    pair_recv,
+    z_send,
+    z_recv,
+    two_send,
+    two_recv,
+    three_send,
+    three_recv,
+    sib_send,
+    sib_recv,
+    red_send,
+    red_recv,
+):
+    live, padded, zs, width, half, experts = sizes
+    live = live + -live % 8
+    quarter = half // 2
+    ep = lax.axis_index("ep")
+    y = lax.axis_index("tp")
+    c = lax.rem(ep, 2)
+    x = lax.rem(ep // 2, 2)
+    z = ep // 4
+
+    def device(zi, xi, ci, yi):
+        return {"ep": zi * 4 + xi * 2 + ci, "tp": yi}
+
+    sibling = device(z, x, 1 - c, y)
+    across_y = device(z, x, c, 1 - y)
+    across_x = device(z, 1 - x, c, y)
+    axis_two = device(z, x + (1 - c) * (1 - 2 * x), c, y + c * (1 - 2 * y))
+    axis_three = device(z, x + c * (1 - 2 * x), c, y + (1 - c) * (1 - 2 * y))
+
+    loads = [
+        pltpu.make_async_copy(gate_hbm.at[0], gate_w, load_sem.at[0]),
+        pltpu.make_async_copy(up_hbm.at[0], up_w, load_sem.at[1]),
+        pltpu.make_async_copy(down_hbm.at[0], down_w, load_sem.at[2]),
+    ]
+    for load in loads:
+        load.start()
+
+    barrier = pltpu.get_barrier_semaphore()
+    partners = [sibling, across_y, across_x] + [
+        device(lax.rem(z + d, zs), x, c, y) for d in range(1, zs)
+    ]
+    for partner in partners:
+        pl.semaphore_signal(
+            barrier, inc=1, device_id=partner, device_id_type=pl.DeviceIdType.MESH
+        )
+    pl.semaphore_wait(barrier, len(partners))
+
+    pending = []
+
+    def send(src, dst, send_sem, recv_sem, target):
+        copy = pltpu.make_async_remote_copy(
+            src_ref=src,
+            dst_ref=dst,
+            send_sem=send_sem,
+            recv_sem=recv_sem,
+            device_id=target,
+            device_id_type=pl.DeviceIdType.MESH,
+        )
+        copy.start()
+        pending.append(copy)
+        return copy
+
+    first = send(part_ref, part_in, pair_send.at[0], pair_recv.at[0], across_y)
+    first.wait_recv()
+    values = (hid_ref[...].astype(jnp.float32) + (part_ref[...] + part_in[...])).astype(
+        jnp.bfloat16
+    )
+    values = values.astype(jnp.float32)
+    resid[...] = values
+    inverse = lax.rsqrt(jnp.sum(values * values, axis=1, keepdims=True) / width + norm_eps)
+    mine = pl.ds(pl.multiple_of(y * half, half), half)
+    normed = resid[:, mine] * inverse * gain_ref[:, mine]
+    rows[y, x, z, c, :, :half] = normed.astype(jnp.bfloat16)
+    rows[y, x, z, c, :, half:] = wts_ref[...]
+
+    def block(yi, xi, zi):
+        return rows.at[yi, xi, zi, c, pl.ds(0, live), :]
+
+    def share(where, slot, send_sem, recv_sem, target):
+        ref = block(*where)
+        return send(ref, ref, send_sem.at[slot], recv_sem.at[slot], target)
+
+    from_z, from_two, from_three, from_core = [], [], [], []
+    me = (y, x, z)
+    for d in range(1, zs):
+        from_z.append(
+            share(me, d - 1, z_send, z_recv, device(lax.rem(z + d, zs), x, c, y))
+        )
+    for d in range(zs):
+        if d > 0:
+            from_z[d - 1].wait_recv()
+        where = (y, x, lax.rem(z - d + zs, zs))
+        from_two.append(share(where, d, two_send, two_recv, axis_two))
+        from_three.append(share(where, d, three_send, three_recv, axis_three))
+        from_core.append(share(where, d, sib_send, sib_recv, sibling))
+    x_two, y_two = x + (1 - c) * (1 - 2 * x), y + c * (1 - 2 * y)
+    for d in range(zs):
+        from_two[d].wait_recv()
+        where = (y_two, x_two, lax.rem(z - d + zs, zs))
+        from_three.append(share(where, zs + d, three_send, three_recv, axis_three))
+        from_core.append(share(where, zs + d, sib_send, sib_recv, sibling))
+    x_three, y_three = x + c * (1 - 2 * x), y + (1 - c) * (1 - 2 * y)
+    for d in range(2 * zs):
+        from_three[d].wait_recv()
+        zi = lax.rem(z - d + 2 * zs, zs)
+        where = (y_three, x_three, zi) if d < zs else (1 - y, 1 - x, zi)
+        from_core.append(share(where, 2 * zs + d, sib_send, sib_recv, sibling))
+    for copy in from_core:
+        copy.wait_recv()
+    for load in loads:
+        load.wait()
+
+    count = 4 * zs * padded
+    gate_act, up_act = 0.0, 0.0
+    for yi in range(2):
+        taken = rows[yi, :, :, :, :, :half].reshape(count, half)
+        depth = slice(yi * half, (yi + 1) * half)
+        gate_act += jnp.dot(taken, gate_w[depth], preferred_element_type=jnp.float32)
+        up_act += jnp.dot(taken, up_w[depth], preferred_element_type=jnp.float32)
+    hidden = (jax.nn.silu(gate_act) * up_act).astype(jnp.bfloat16)
+    coded = rows[0, :, :, :, :, half:].reshape(count, -1).astype(jnp.float32)
+    lane = lax.broadcasted_iota(jnp.int32, coded.shape, 1)
+    named = (lane == ep) | (lane == ep + experts)
+    weight = jnp.sum(jnp.where(named, coded, 0.0), axis=1, keepdims=True)
+
+    def piece(yi, ci):
+        columns = pl.ds(pl.multiple_of(yi * half + ci * quarter, quarter), quarter)
+        result = jnp.dot(hidden, down_w[:, columns], preferred_element_type=jnp.float32)
+        return (result * weight).reshape(2, zs, 2, padded, quarter)
+
+    halves = []
+    for yi in range(2):
+        for_sib[yi] = piece(yi, 1 - c).astype(jnp.bfloat16)
+        halves.append(
+            send(for_sib.at[yi], from_sib.at[yi], red_send.at[yi], red_recv.at[yi], sibling)
+        )
+    for yi in range(2):
+        own[yi] = piece(yi, c)
+    for copy in halves:
+        copy.wait_recv()
+
+    one = y + c * (x - y)
+    two = x + c * (y - x)
+
+    def summed(fi, si):
+        yi, xi = fi + c * (si - fi), si + c * (fi - si)
+        return own[yi, xi] + from_sib[yi, xi].astype(jnp.float32)
+
+    for si in range(2):
+        stage_a[si] = summed(1 - one, si).astype(jnp.bfloat16)
+    to_first = send(stage_a, recv_a, red_send.at[2], red_recv.at[2], axis_three)
+    to_first.wait_recv()
+    stage_b[...] = (summed(one, 1 - two) + recv_a[1 - two].astype(jnp.float32)).astype(
+        jnp.bfloat16
+    )
+    to_second = send(stage_b, recv_b, red_send.at[3], red_recv.at[3], axis_two)
+    kept = summed(one, two) + recv_a[two].astype(jnp.float32)
+    to_second.wait_recv()
+    own[0, 0] = kept + recv_b[...].astype(jnp.float32)
+    stage_c[...] = own[0, 0].astype(jnp.bfloat16)
+    along_z = []
+    for d in range(1, zs):
+        zi = lax.rem(z + d, zs)
+        along_z.append(
+            send(
+                stage_c.at[zi, :, pl.ds(0, live), :],
+                recv_c.at[d - 1, :, pl.ds(0, live), :],
+                red_send.at[3 + d],
+                red_recv.at[3 + d],
+                device(zi, x, c, y),
+            )
+        )
+    total = own[0, 0, z]
+    for d in range(1, zs):
+        along_z[d - 1].wait_recv()
+        total = total + recv_c[d - 1].astype(jnp.float32)
+    stage_d[...] = total
+    last = send(
+        stage_d.at[1 - c], recv_d, red_send.at[3 + zs], red_recv.at[3 + zs], sibling
+    )
+    near = pl.multiple_of(c * quarter, quarter)
+    far = pl.multiple_of((1 - c) * quarter, quarter)
+    base = pl.multiple_of(y * half, half)
+    out_ref[:, pl.ds(near, quarter)] = (
+        resid[:, pl.ds(pl.multiple_of(base + near, quarter), quarter)] + stage_d[c]
+    ).astype(out_ref.dtype)
+    last.wait_recv()
+    out_ref[:, pl.ds(far, quarter)] = (
+        resid[:, pl.ds(pl.multiple_of(base + far, quarter), quarter)] + recv_d[...]
+    ).astype(out_ref.dtype)
+    for copy in pending:
+        copy.wait_send()
+
+
+def expert_layer(
+    partial_out, gathered, ffn_gain, coded, expert_gate, expert_up, expert_down, live, ep_size
+):
+    padded, width = partial_out.shape
+    half = width // 2
+    zs = ep_size // 4
+    blocks = (2, zs, 2, padded, half // 2)
+    bf16, f32 = jnp.bfloat16, jnp.float32
+    vmem = pl.BlockSpec(memory_space=pltpu.VMEM)
+    hbm = pl.BlockSpec(memory_space=pl.ANY)
+    dma = pltpu.SemaphoreType.DMA
+    sizes = (live, padded, zs, width, half, ep_size)
+    return pl.pallas_call(
+        functools.partial(experts_kernel, sizes),
+        out_shape=jax.ShapeDtypeStruct((padded, half), bf16),
+        in_specs=[vmem] * 4 + [hbm] * 3,
+        out_specs=vmem,
+        scratch_shapes=[
+            pltpu.VMEM(expert_gate.shape[1:], bf16),
+            pltpu.VMEM(expert_up.shape[1:], bf16),
+            pltpu.VMEM(expert_down.shape[1:], bf16),
+            pltpu.VMEM((padded, width), f32),
+            pltpu.VMEM((padded, width), f32),
+            pltpu.VMEM((2, 2, zs, 2, padded, half + coded.shape[1]), bf16),
+            pltpu.VMEM((2,) + blocks, f32),
+            pltpu.VMEM((2,) + blocks, bf16),
+            pltpu.VMEM((2,) + blocks, bf16),
+            pltpu.VMEM(blocks, bf16),
+            pltpu.VMEM(blocks, bf16),
+            pltpu.VMEM(blocks[1:], bf16),
+            pltpu.VMEM(blocks[1:], bf16),
+            pltpu.VMEM(blocks[1:], bf16),
+            pltpu.VMEM((zs - 1,) + blocks[2:], bf16),
+            pltpu.VMEM(blocks[2:], f32),
+            pltpu.VMEM(blocks[3:], f32),
+            dma((3,)),
+            dma((1,)),
+            dma((1,)),
+            dma((zs - 1,)),
+            dma((zs - 1,)),
+            dma((zs,)),
+            dma((zs,)),
+            dma((2 * zs,)),
+            dma((2 * zs,)),
+            dma((4 * zs,)),
+            dma((4 * zs,)),
+            dma((4 + zs,)),
+            dma((4 + zs,)),
+        ],
+        compiler_params=pltpu.CompilerParams(
+            collective_id=0, has_side_effects=True, vmem_limit_bytes=60 * 1024 * 1024
+        ),
+    )(partial_out, gathered, ffn_gain, coded, expert_gate, expert_up, expert_down)
+
+
+def dense_shards(
+    hidden_in,
+    attn_gain,
+    w_query,
+    w_key,
+    w_value,
+    break_bias,
+    key_cache,
+    value_cache,
+    lengths,
+    w_out,
+    ffn_gain,
+    route_ids,
+    route_scores,
+    expert_gate,
+    expert_up,
+    expert_down,
+):
+    gathered = lax.all_gather(hidden_in, "tp", axis=1, tiled=True)
+    normed_attn = rms_norm(gathered, attn_gain)
+    queries = project_rows(normed_attn, w_query)
+    new_keys = project_rows(normed_attn, w_key)
+    new_values = project_rows(normed_attn, w_value)
+    attended = stick_breaking(queries, key_cache, value_cache, lengths, break_bias)
+    live = hidden_in.shape[0]
+    extra = ((0, -live % 16), (0, 0))
+    partial_out = jnp.dot(jnp.pad(attended, extra), w_out, preferred_element_type=jnp.float32)
+    experts = lax.axis_size("ep")
+    route_weight = route_scores / jnp.sum(route_scores, axis=1, keepdims=True)
+    named = route_ids[:, :, None] == jnp.arange(experts, dtype=jnp.int32)[None, None, :]
+    dense = jnp.sum(jnp.where(named, route_weight[:, :, None], 0.0), axis=1)
+    high = lax.reduce_precision(dense, 8, 7)
+    coded = jnp.concatenate([high, dense - high], axis=1).astype(jnp.bfloat16)
+    coded = jnp.pad(coded, (extra[0], (0, -coded.shape[1] % 128)))
+    hidden_out = expert_layer(
+        partial_out,
+        jnp.pad(gathered, extra),
+        ffn_gain[None, :],
+        coded,
+        expert_gate,
+        expert_up,
+        expert_down,
+        live,
+        experts,
+    )
+    return (hidden_out[:live], new_keys, new_values)
+
+
 def solution(mesh):
+    ep_size, tp_size = mesh.shape["ep"], mesh.shape["tp"]
+    fits = tp_size == 2 and ep_size % 4 == 0 and 8 <= ep_size <= 16
+    body = dense_shards if fits else shards
     return jax.shard_map(
-        shards,
+        body,
         mesh=mesh,
         in_specs=(
             P("ep", "tp"),

time: 145 us -> 74.9 us (0.52)
  Pallas kernels: 0 us -> 49 us
  waiting for transfers between devices: 40.6 us -> 0 us
  blocking collectives: 44.7 us -> 5.99 us
  between operations: 14.3 us -> 0.71 us
  other arithmetic: 15.3 us -> 4.38 us
  starting transfers between devices: 5.75 us -> 0 us
  local copies, waits for them, and re-layouts: 9.72 us -> 4.3 us
  matrix products: 13.6 us -> 9.74 us
    pallas_call x0 -> x1, Pallas kernels: none -> 49 us  [expert_layer(): pl.pallas_call(functools.partial(experts_kernel, sizes), out_shape=jax.Sh...]
    reduce_scatter x2 -> x0, waiting for transfers between devices: 29.3 us -> none  [the longest x1 18.5 us: shards(): lax.psum_scatter(partial_value.astype(jnp.float32).astype(jnp.bfloat16),...]
    all_to_all x1 -> x0, blocking collectives: 19.8 us -> none  [shards(): lax.all_to_all(outgoing.astype(jnp.bfloat16).reshape(experts, capacity, n...]
    all_gather x2 -> x1, blocking collectives: 19.9 us -> 5.99 us  [dense_shards(): gathered = lax.all_gather(hidden_in, 'tp', axis=1, tiled=True)]
    all_to_all x1 -> x0, waiting for transfers between devices: 11.2 us -> none  [shards(): lax.all_to_all(summed, 'ep', split_axis=0, concat_axis=0, tiled=True)]
    another operation x4 -> x1, other arithmetic: 10.3 us -> 0.01 us
    all_to_all x1 -> x0, starting transfers between devices: 5.67 us -> none  [shards(): lax.all_to_all(summed, 'ep', split_axis=0, concat_axis=0, tiled=True)]
    dot_general x4, matrix products: 6.47 us -> 1.54 us  [the longest x1 0.9 us: dense_shards(): jnp.dot(jnp.pad(attended, extra), w_out, preferred_element_type=jnp.float32)]
  transfers between devices with their start and end apart: 3 -> 0, of which waited for: 3 -> 0; matrix products, arithmetic and copies ran while one was open for 4% -> 0% of each run, Pallas kernels for 0% -> 0%
where the time goes in v1:
time: 74.9 us; the launch traced here: 74.1 us
  Pallas kernels  49 us (65%)
  matrix products  9.74 us (13%)
  blocking collectives  5.99 us (8%)
  other arithmetic  4.38 us (6%)
  local copies, waits for them, and re-layouts  4.3 us (6%)
    pallas_call x1, Pallas kernels, expert_layer(): pl.pallas_call(functools.partial(experts_kernel, sizes), out_shape=jax.Sh...  49 us
    all_gather x1, blocking collectives, dense_shards(): gathered = lax.all_gather(hidden_in, 'tp', axis=1, tiled=True)  5.99 us
    dot_general x3, matrix products, project_rows(): lax.dot_general(normed, weight, (((1,), (1,)), ((), ())), preferred_eleme...  5.25 us
    dot_general x1, matrix products, stick_breaking(): jnp.einsum('shl,shdl->shd', stick, v_heads, preferred_element_type=jnp.fl...  2.51 us
    unnamed x6, local copies, waits for them, and re-layouts  1.75 us

profile of v1, /device:TPU:0, one launch (start us, length us, event | category | flops | bytes accessed | tf_op | source)
XLA Modules:
  0.0 74.1 jit_solution(16112163883301163693)
XLA Ops:
  0.6 0.0 copy-start
  0.6 1.7 %copy-done = bf16[20,128,512]{2,1,0:T(8,128)(2,1)S(1)} copy-done((bf16[20,128,512]{2,1,0:T(8,128)(2,1)S(1)}, bf16[20,128,512]{2,1,0:T(8,128)(2,1)}, u32[]{:S(2)}) %copy-start) | copy-done | bytes 2621464
  2.4 0.7 reduce_sum.28
  3.1 0.7 broadcast_divide_fusion
  3.8 0.7 select_reduce_fusion
  4.5 0.1 copy.24
  4.6 0.0 copy-start.2
  4.6 0.1 copy.23
  4.7 0.7 fusion.21.wts_ref
  5.4 0.7 iota_compare_fusion.5
  6.1 6.0 %all_gather.3 = bf16[20,2048]{1,0:T(8,128)(2,1)S(1)} all-gather(bf16[20,1024]{1,0:T(8,128)(2,1)} %param.16), channel_id=1, replica_groups=mesh['ep'=16,'tp'=2] {'tp'}, dimensions={1}, use_global_device_ids=true | all-gather | bytes 122880 | tf_op jit(solution)/shard_map/all_gather | solution.py:446
  12.1 0.1 fusion.1
  12.2 2.0 %convolution_convert_fusion.1 = bf16[20,128]{1,0:T(8,128)(2,1)} fusion(bf16[128,2048]{1,0:T(8,128)(2,1)} %param.19, bf16[20,2048]{1,0:T(8,128)(2,1)S(1)} %all_gather.3, f32[2048]{0:T(1024)} %param.17, f32[20]{0:T(128)S(1)} %add_rsqrt_fusion), kind=kOutput, calls=%fused_computation.3 | convolution fusion | flops 10652160 | bytes 619600 | tf_op jit(solution)/shard_map/dot_general | solution.py:23
  14.2 2.0 %convolution_convert_fusion = bf16[20,128]{1,0:T(8,128)(2,1)} fusion(bf16[128,2048]{1,0:T(8,128)(2,1)} %param.20, bf16[20,2048]{1,0:T(8,128)(2,1)S(1)} %all_gather.3, f32[2048]{0:T(1024)} %param.17, f32[20]{0:T(128)S(1)} %add_rsqrt_fusion), kind=kOutput, calls=%fused_computation.2 | convolution fusion | flops 10652160 | bytes 619600 | tf_op jit(solution)/shard_map/dot_general | solution.py:23
  16.1 1.3 %convolution_convert_fusion.2 = bf16[20,128]{1,0:T(8,128)(2,1)S(1)} fusion(bf16[128,2048]{1,0:T(8,128)(2,1)} %param.18, bf16[20,2048]{1,0:T(8,128)(2,1)S(1)} %all_gather.3, f32[2048]{0:T(1024)} %param.17, f32[20]{0:T(128)S(1)} %add_rsqrt_fusion), kind=kOutput, calls=%fused_computation.4 | convolution fusion | flops 10652160 | bytes 619600 | tf_op jit(solution)/shard_map/dot_general | solution.py:23
  17.5 0.1 reshape.63
  17.6 0.7 pad.13.hid_ref
  18.2 0.4 fusion.29
  18.7 0.0 copy-done.2
  18.7 0.0 copy-start.1
  18.7 0.3 fusion.8
  19.0 0.1 reshape.55
  19.1 0.2 fusion
  19.3 0.2 convolution_add_fusion.1
  19.5 0.2 convolution_add_fusion
  19.8 0.4 fusion.15
  20.2 2.5 %fusion.10 = f32[20,2,1,64]{3,2,1,0:T(1,128)S(1)} fusion(bf16[20,2,64,512]{3,2,1,0:T(8,128)(2,1)} %bitcast.25, bf16[20,2,512,1]{2,1,0,3:T(2,128)(2,1)S(1)} %fusion.15), kind=kOutput, calls=%fused_computation.21 | convolution fusion | flops 2621440 | bytes 2672640 | tf_op jit(solution)/shard_map/shl,shdl->shd/dot_general | solution.py:56
  22.7 0.1 convert_element_type.57
  22.8 0.0 copy-done.1
  22.8 0.9 %fusion.22.part_ref = f32[32,2048]{1,0:T(8,128)} fusion(bf16[128,2048]{1,0:T(8,128)(2,1)S(1)} %copy-done.1, bf16[20,128]{1,0:T(8,128)(2,1)S(1)} %convert_element_type.57), kind=kOutput, calls=%fused_computation.41 | convolution fusion | flops 16777216 | bytes 791552 | tf_op jit(solution)/shard_map/dot_general | solution.py:454
  23.7 49.0 %shard_map.175 = bf16[32,1024]{1,0:T(8,128)(2,1)} custom-call(f32[32,2048]{1,0:T(8,128)} %fusion.22.part_ref, bf16[32,2048]{1,0:T(8,128)(2,1)} %pad.13.hid_ref, f32[1,2048]{1,0:T(1,128)} %bitcast.24, bf16[32,128]{1,0:T(8,128)(2,1)} %fusion.21.wts_ref, bf16[1,2048,256]{2,1,0:T(8,128)(2,1)} %gate_hbm.1, bf16[1,2048,256]{2,1,0:T(8,128)(2,1)} %up_hbm.1, ...), custom_call_target="tpu_custom_call" | custom-call | tf_op jit(solution)/shard_map/pallas_call | solution.py:385
  72.7 1.4 %slice.3 = bf16[20,1024]{1,0:T(8,128)(2,1)} slice(bf16[32,1024]{1,0:T(8,128)(2,1)} %shard_map.175), slice={[0:20], [0:1024]} | slice | bytes 81920 | tf_op jit(solution)/shard_map/slice | solution.py:473
  (5 shorter events, 0.1 us)
Async XLA Ops:
  0.6 1.7 %copy-start = (bf16[20,128,512]{2,1,0:T(8,128)(2,1)S(1)}, bf16[20,128,512]{2,1,0:T(8,128)(2,1)}, u32[]{:S(2)}) copy-start(bf16[20,128,512]{2,1,0:T(8,128)(2,1)} %param.22) | copy-start | bytes 7864324
  4.6 14.1 %copy-start.2 = (f32[2]{0:T(128)S(1)}, f32[2]{0:T(128)}, u32[]{:S(2)}) copy-start(f32[2]{0:T(128)} %param.21) | copy-start | bytes 28
  18.7 4.1 %copy-start.1 = (bf16[128,2048]{1,0:T(8,128)(2,1)S(1)}, bf16[128,2048]{1,0:T(8,128)(2,1)}, u32[]{:S(2)}) copy-start(bf16[128,2048]{1,0:T(8,128)(2,1)} %param.25) | copy-start | bytes 1572868

commit v2 on v1

--- a/solution.py
+++ b/solution.py
@@ -23,20 +23,6 @@
     return lax.dot_general(
         normed, weight, (((1,), (1,)), ((), ())), preferred_element_type=jnp.float32
     ).astype(jnp.bfloat16)
-
-
-def sum_later(values):
-    span = values.shape[-1]
-    flat = values.reshape(-1, span)
-    row = lax.broadcasted_iota(jnp.int32, (span, span), 0)
-    col = lax.broadcasted_iota(jnp.int32, (span, span), 1)
-    later = (row > col).astype(jnp.bfloat16)
-    total, rest = 0.0, flat
-    for _ in range(3):
-        term = rest.astype(jnp.bfloat16)
-        rest = rest - term.astype(jnp.float32)
-        total = total + jnp.dot(term, later, preferred_element_type=jnp.float32)
-    return total.reshape(values.shape)
 
 
 def stick_breaking(queries, key_block, value_block, lengths, break_bias):
@@ -49,7 +35,7 @@
     position = jnp.arange(key_block.shape[2], dtype=jnp.int32)
     visible = (position[None, :] < lengths[:, None])[:, None, :]
     log_keep = jnp.where(visible, jax.nn.log_sigmoid(-logit), 0.0)
-    later_sum = sum_later(log_keep)
+    later_sum = lax.cumsum(log_keep, axis=2, reverse=True) - log_keep
     stick = jnp.where(visible, jnp.exp(jax.nn.log_sigmoid(logit) + later_sum), 0.0).astype(
         jnp.bfloat16
     )
@@ -146,20 +132,40 @@
     return (hidden_out, new_keys, new_values)
 
 
-def experts_kernel(
+def layer_kernel(
     sizes,
-    part_ref,
     hid_ref,
+    attn_gain_ref,
+    bias_ref,
+    lengths_ref,
     gain_ref,
-    wts_ref,
+    ids_ref,
+    scores_ref,
+    wq_hbm,
+    wk_hbm,
+    wv_hbm,
+    key_hbm,
+    value_hbm,
+    wo_hbm,
     gate_hbm,
     up_hbm,
     down_hbm,
     out_ref,
+    new_key_ref,
+    new_value_ref,
+    w_in,
+    key_c,
+    value_c,
+    wo_full,
     gate_w,
     up_w,
     down_w,
-    part_in,
+    hid_both,
+    normed_in,
+    logits,
+    spans,
+    stick,
+    att_both,
     resid,
     rows,
     own,
@@ -186,10 +192,15 @@
     sib_recv,
     red_send,
     red_recv,
+    a_send,
+    a_recv,
+    b_send,
+    b_recv,
 ):
-    live, padded, zs, width, half, experts = sizes
-    live = live + -live % 8
+    tokens, padded, zs, width, half, experts, heads = sizes
+    live = tokens + -tokens % 8
     quarter = half // 2
+    columns_in = heads * HEAD_DIM
     ep = lax.axis_index("ep")
     y = lax.axis_index("tp")
     c = lax.rem(ep, 2)
@@ -205,10 +216,19 @@
     axis_two = device(z, x + (1 - c) * (1 - 2 * x), c, y + c * (1 - 2 * y))
     axis_three = device(z, x + c * (1 - 2 * x), c, y + (1 - c) * (1 - 2 * y))
 
+    sources = [
+        (wq_hbm, w_in.at[0]),
+        (wk_hbm, w_in.at[1]),
+        (wv_hbm, w_in.at[2]),
+        (key_hbm, key_c),
+        (value_hbm, value_c),
+        (wo_hbm, wo_full.at[y]),
+        (gate_hbm.at[0], gate_w),
+        (up_hbm.at[0], up_w),
+        (down_hbm.at[0], down_w),
+    ]
     loads = [
-        pltpu.make_async_copy(gate_hbm.at[0], gate_w, load_sem.at[0]),
-        pltpu.make_async_copy(up_hbm.at[0], up_w, load_sem.at[1]),
-        pltpu.make_async_copy(down_hbm.at[0], down_w, load_sem.at[2]),
+        pltpu.make_async_copy(src, dst, load_sem.at[i]) for i, (src, dst) in enumerate(sources)
     ]
     for load in loads:
         load.start()
@@ -238,18 +258,121 @@
         pending.append(copy)
         return copy
 
-    first = send(part_ref, part_in, pair_send.at[0], pair_recv.at[0], across_y)
-    first.wait_recv()
-    values = (hid_ref[...].astype(jnp.float32) + (part_ref[...] + part_in[...])).astype(
+    give = send(hid_ref, hid_both.at[y], pair_send.at[0], pair_recv.at[0], across_y)
+    wo_rows = columns_in // 2
+    wo_part = pl.ds(pl.multiple_of(c * wo_rows, wo_rows), wo_rows)
+    give_wo = send(
+        wo_hbm.at[wo_part], wo_full.at[y, wo_part], pair_send.at[1], pair_recv.at[1], across_y
+    )
+    hid_both[y] = hid_ref[...]
+    normed_in[...] = jnp.zeros_like(normed_in)
+
+    scores = scores_ref[...]
+    route_weight = scores / jnp.sum(scores, axis=1, keepdims=True)
+    high = route_weight.astype(jnp.bfloat16).astype(jnp.float32)
+    low = route_weight - high
+    ids = ids_ref[...]
+    extra = rows.shape[-1] - half
+    lane = lax.broadcasted_iota(jnp.int32, (tokens, extra), 1)
+    coded = jnp.zeros((tokens, extra), jnp.float32)
+    for k in range(ids.shape[1]):
+        name = ids[:, k : k + 1]
+        coded += jnp.where(lane == name, high[:, k : k + 1], 0.0)
+        coded += jnp.where(lane == name + experts, low[:, k : k + 1], 0.0)
+    rows[y, x, z, c, :tokens, half:] = coded.astype(jnp.bfloat16)
+
+    give.wait_recv()
+    left = hid_both[0].astype(jnp.float32)
+    right = hid_both[1].astype(jnp.float32)
+    square = jnp.sum(left * left, axis=1, keepdims=True) + jnp.sum(
+        right * right, axis=1, keepdims=True
+    )
+    inverse = lax.rsqrt(square / width + norm_eps)
+    normed_in[:tokens, :half] = (left * inverse * attn_gain_ref[:, :half]).astype(jnp.bfloat16)
+    normed_in[:tokens, half:] = (right * inverse * attn_gain_ref[:, half:]).astype(jnp.bfloat16)
+    for load in loads[:3]:
+        load.wait()
+    across = (((1,), (1,)), ((), ()))
+    q_cols = lax.dot_general(
+        w_in[0], normed_in[...], across, preferred_element_type=jnp.float32
+    )
+    q_cols = q_cols.astype(jnp.bfloat16).astype(jnp.float32)
+    for i, ref in ((1, new_key_ref), (2, new_value_ref)):
+        made = lax.dot_general(
+            normed_in[...], w_in[i], across, preferred_element_type=jnp.float32
+        )
+        ref[...] = made[:tokens].astype(jnp.bfloat16)
+
+    span = key_c.shape[2]
+    q_lane = lax.broadcasted_iota(jnp.int32, q_cols.shape, 1)
+    loads[3].wait()
+
+    def score(t, carry):
+        column = jnp.sum(jnp.where(q_lane == t, q_cols, 0.0), axis=1, keepdims=True)
+        scaled = key_c[t].astype(jnp.float32) * column
+        for h in range(heads):
+            summed_h = jnp.sum(scaled[h * HEAD_DIM : (h + 1) * HEAD_DIM], axis=0, keepdims=True)
+            logits[h, pl.ds(t, 1), :] = summed_h * HEAD_DIM ** (-0.5) + bias_ref[h]
+        spans[pl.ds(t, 1), :] = jnp.full((1, span), lengths_ref[t], jnp.int32)
+        return carry
+
+    lax.fori_loop(0, tokens, score, 0, unroll=2)
+    row = lax.broadcasted_iota(jnp.int32, (span, span), 0)
+    col = lax.broadcasted_iota(jnp.int32, (span, span), 1)
+    later = (row > col).astype(jnp.float32).astype(jnp.bfloat16)
+    position = lax.broadcasted_iota(jnp.int32, (padded, span), 1)
+    visible = position < spans[...]
+    for h in range(heads):
+        logit = logits[h]
+        soft = jnp.log1p(jnp.exp(-jnp.abs(logit)))
+        log_keep = jnp.where(visible, -jnp.maximum(logit, 0.0) - soft, 0.0)
+        total, rest = 0.0, log_keep
+        for _ in range(3):
+            term = rest.astype(jnp.bfloat16)
+            rest = rest - term.astype(jnp.float32)
+            total = total + jnp.dot(term, later, preferred_element_type=jnp.float32)
+        value = jnp.where(visible, jnp.exp(jnp.minimum(logit, 0.0) - soft + total), 0.0)
+        stick[h] = value.astype(jnp.bfloat16).astype(jnp.float32)
+    loads[4].wait()
+    att_lane = lax.broadcasted_iota(jnp.int32, (columns_in, 128), 1)
+
+    def attend(t, gathered):
+        parts = []
+        for h in range(heads):
+            part = value_c[t, h * HEAD_DIM : (h + 1) * HEAD_DIM].astype(jnp.float32)
+            parts.append(
+                jnp.sum(part * stick[h, pl.ds(t, 1), :], axis=1, keepdims=True)
+            )
+        column = jnp.concatenate(parts, axis=0)
+        return jnp.where(att_lane == t, column, gathered)
+
+    gathered = lax.fori_loop(
+        0, tokens, attend, jnp.zeros((columns_in, 128), jnp.float32), unroll=2
+    )
+    att_both[y] = gathered.T[:padded].astype(jnp.bfloat16)
+    give_att = send(
+        att_both.at[y], att_both.at[y], pair_send.at[2], pair_recv.at[2], across_y
+    )
+    give_wo.wait_recv()
+    came = wo_full.at[1 - y, wo_part]
+    share_wo = send(came, came, pair_send.at[3], pair_recv.at[3], sibling)
+    loads[5].wait()
+    share_wo.wait_recv()
+    give_att.wait_recv()
+    mixer = jnp.dot(att_both[0], wo_full[0], preferred_element_type=jnp.float32)
+    mixer += jnp.dot(att_both[1], wo_full[1], preferred_element_type=jnp.float32)
+    left = (left + mixer[:tokens, :half]).astype(jnp.bfloat16).astype(jnp.float32)
+    right = (right + mixer[:tokens, half:]).astype(jnp.bfloat16).astype(jnp.float32)
+    square = jnp.sum(left * left, axis=1, keepdims=True) + jnp.sum(
+        right * right, axis=1, keepdims=True
+    )
+    inverse = lax.rsqrt(square / width + norm_eps)
+    mine = pl.ds(pl.multiple_of(y * half, half), half)
+    values = jnp.where(y == 0, left, right)
+    resid[...] = values
+    rows[y, x, z, c, :tokens, :half] = (values * inverse * gain_ref[:, mine]).astype(
         jnp.bfloat16
     )
-    values = values.astype(jnp.float32)
-    resid[...] = values
-    inverse = lax.rsqrt(jnp.sum(values * values, axis=1, keepdims=True) / width + norm_eps)
-    mine = pl.ds(pl.multiple_of(y * half, half), half)
-    normed = resid[:, mine] * inverse * gain_ref[:, mine]
-    rows[y, x, z, c, :, :half] = normed.astype(jnp.bfloat16)
-    rows[y, x, z, c, :, half:] = wts_ref[...]
 
     def block(yi, xi, zi):
         return rows.at[yi, xi, zi, c, pl.ds(0, live), :]
@@ -285,7 +408,7 @@
         from_core.append(share(where, 2 * zs + d, sib_send, sib_recv, sibling))
     for copy in from_core:
         copy.wait_recv()
-    for load in loads:
+    for load in loads[6:]:
         load.wait()
 
     count = 4 * zs * padded
@@ -307,10 +430,17 @@
         return (result * weight).reshape(2, zs, 2, padded, quarter)
 
     halves = []
+    some = (slice(None), slice(None), slice(None), pl.ds(0, live), slice(None))
     for yi in range(2):
         for_sib[yi] = piece(yi, 1 - c).astype(jnp.bfloat16)
         halves.append(
-            send(for_sib.at[yi], from_sib.at[yi], red_send.at[yi], red_recv.at[yi], sibling)
+            send(
+                for_sib.at[(yi,) + some],
+                from_sib.at[(yi,) + some],
+                red_send.at[yi],
+                red_recv.at[yi],
+                sibling,
+            )
         )
     for yi in range(2):
         own[yi] = piece(yi, c)
@@ -320,109 +450,62 @@
     one = y + c * (x - y)
     two = x + c * (y - x)
 
-    def summed(fi, si):
+    def summed(fi, si, zi):
         yi, xi = fi + c * (si - fi), si + c * (fi - si)
-        return own[yi, xi] + from_sib[yi, xi].astype(jnp.float32)
-
-    for si in range(2):
-        stage_a[si] = summed(1 - one, si).astype(jnp.bfloat16)
-    to_first = send(stage_a, recv_a, red_send.at[2], red_recv.at[2], axis_three)
-    to_first.wait_recv()
-    stage_b[...] = (summed(one, 1 - two) + recv_a[1 - two].astype(jnp.float32)).astype(
-        jnp.bfloat16
-    )
-    to_second = send(stage_b, recv_b, red_send.at[3], red_recv.at[3], axis_two)
-    kept = summed(one, two) + recv_a[two].astype(jnp.float32)
-    to_second.wait_recv()
-    own[0, 0] = kept + recv_b[...].astype(jnp.float32)
-    stage_c[...] = own[0, 0].astype(jnp.bfloat16)
-    along_z = []
-    for d in range(1, zs):
-        zi = lax.rem(z + d, zs)
-        along_z.append(
-            send(
-                stage_c.at[zi, :, pl.ds(0, live), :],
-                recv_c.at[d - 1, :, pl.ds(0, live), :],
-                red_send.at[3 + d],
-                red_recv.at[3 + d],
-                device(zi, x, c, y),
+        return own[yi, xi, zi] + from_sib[yi, xi, zi].astype(jnp.float32)
+
+    order = [lax.rem(z + d, zs) for d in list(range(1, zs)) + [0]]
+    cut = (slice(None), pl.ds(0, live), slice(None))
+    to_first, to_second, along_z = [], [], []
+    for j, si in enumerate((1 - two, two)):
+        for i, zi in enumerate(order):
+            stage_a[si, zi] = summed(1 - one, si, zi).astype(jnp.bfloat16)
+            at = (si, zi) + cut
+            slot = j * zs + i
+            to_first.append(
+                send(stage_a.at[at], recv_a.at[at], a_send.at[slot], a_recv.at[slot], axis_three)
             )
+    for i, zi in enumerate(order):
+        to_first[i].wait_recv()
+        stage_b[zi] = (
+            summed(one, 1 - two, zi) + recv_a[1 - two, zi].astype(jnp.float32)
+        ).astype(jnp.bfloat16)
+        at = (zi,) + cut
+        to_second.append(
+            send(stage_b.at[at], recv_b.at[at], b_send.at[i], b_recv.at[i], axis_two)
         )
-    total = own[0, 0, z]
-    for d in range(1, zs):
-        along_z[d - 1].wait_recv()
-        total = total + recv_c[d - 1].astype(jnp.float32)
+    for i, zi in enumerate(order):
+        to_first[zs + i].wait_recv()
+        to_second[i].wait_recv()
+        kept = (
+            summed(one, two, zi)
+            + recv_a[two, zi].astype(jnp.float32)
+            + recv_b[zi].astype(jnp.float32)
+        )
+        if i < zs - 1:
+            stage_c[zi] = kept.astype(jnp.bfloat16)
+            along_z.append(
+                send(
+                    stage_c.at[(zi,) + cut],
+                    recv_c.at[(i,) + cut],
+                    red_send.at[3 + i],
+                    red_recv.at[3 + i],
+                    device(zi, x, c, y),
+                )
+            )
+    total = kept
+    for i in range(zs - 1):
+        along_z[i].wait_recv()
+        total = total + recv_c[i].astype(jnp.float32)
     stage_d[...] = total
-    last = send(
-        stage_d.at[1 - c], recv_d, red_send.at[3 + zs], red_recv.at[3 + zs], sibling
-    )
-    near = pl.multiple_of(c * quarter, quarter)
-    far = pl.multiple_of((1 - c) * quarter, quarter)
-    base = pl.multiple_of(y * half, half)
-    out_ref[:, pl.ds(near, quarter)] = (
-        resid[:, pl.ds(pl.multiple_of(base + near, quarter), quarter)] + stage_d[c]
-    ).astype(out_ref.dtype)
+    last = send(stage_d.at[1 - c], recv_d, red_send.at[2], red_recv.at[2], sibling)
+    near = pl.ds(pl.multiple_of(c * quarter, quarter), quarter)
+    far = pl.ds(pl.multiple_of((1 - c) * quarter, quarter), quarter)
+    out_ref[:, near] = (resid[:, near] + stage_d[c, :tokens]).astype(out_ref.dtype)
     last.wait_recv()
-    out_ref[:, pl.ds(far, quarter)] = (
-        resid[:, pl.ds(pl.multiple_of(base + far, quarter), quarter)] + recv_d[...]
-    ).astype(out_ref.dtype)
+    out_ref[:, far] = (resid[:, far] + recv_d[:tokens]).astype(out_ref.dtype)
     for copy in pending:
         copy.wait_send()
-
-
-def expert_layer(
-    partial_out, gathered, ffn_gain, coded, expert_gate, expert_up, expert_down, live, ep_size
-):
-    padded, width = partial_out.shape
-    half = width // 2
-    zs = ep_size // 4
-    blocks = (2, zs, 2, padded, half // 2)
-    bf16, f32 = jnp.bfloat16, jnp.float32
-    vmem = pl.BlockSpec(memory_space=pltpu.VMEM)
-    hbm = pl.BlockSpec(memory_space=pl.ANY)
-    dma = pltpu.SemaphoreType.DMA
-    sizes = (live, padded, zs, width, half, ep_size)
-    return pl.pallas_call(
-        functools.partial(experts_kernel, sizes),
-        out_shape=jax.ShapeDtypeStruct((padded, half), bf16),
-        in_specs=[vmem] * 4 + [hbm] * 3,
-        out_specs=vmem,
-        scratch_shapes=[
-            pltpu.VMEM(expert_gate.shape[1:], bf16),
-            pltpu.VMEM(expert_up.shape[1:], bf16),
-            pltpu.VMEM(expert_down.shape[1:], bf16),
-            pltpu.VMEM((padded, width), f32),
-            pltpu.VMEM((padded, width), f32),
-            pltpu.VMEM((2, 2, zs, 2, padded, half + coded.shape[1]), bf16),
-            pltpu.VMEM((2,) + blocks, f32),
-            pltpu.VMEM((2,) + blocks, bf16),
-            pltpu.VMEM((2,) + blocks, bf16),
-            pltpu.VMEM(blocks, bf16),
-            pltpu.VMEM(blocks, bf16),
-            pltpu.VMEM(blocks[1:], bf16),
-            pltpu.VMEM(blocks[1:], bf16),
-            pltpu.VMEM(blocks[1:], bf16),
-            pltpu.VMEM((zs - 1,) + blocks[2:], bf16),
-            pltpu.VMEM(blocks[2:], f32),
-            pltpu.VMEM(blocks[3:], f32),
-            dma((3,)),
-            dma((1,)),
-            dma((1,)),
-            dma((zs - 1,)),
-            dma((zs - 1,)),
-            dma((zs,)),
-            dma((zs,)),
-            dma((2 * zs,)),
-            dma((2 * zs,)),
-            dma((4 * zs,)),
-            dma((4 * zs,)),
-            dma((4 + zs,)),
-            dma((4 + zs,)),
-        ],
-        compiler_params=pltpu.CompilerParams(
-            collective_id=0, has_side_effects=True, vmem_limit_bytes=60 * 1024 * 1024
-        ),
-    )(partial_out, gathered, ffn_gain, coded, expert_gate, expert_up, expert_down)
 
 
 def dense_shards(
@@ -443,34 +526,79 @@
     expert_up,
     expert_down,
 ):
-    gathered = lax.all_gather(hidden_in, "tp", axis=1, tiled=True)
-    normed_attn = rms_norm(gathered, attn_gain)
-    queries = project_rows(normed_attn, w_query)
-    new_keys = project_rows(normed_attn, w_key)
-    new_values = project_rows(normed_attn, w_value)
-    attended = stick_breaking(queries, key_cache, value_cache, lengths, break_bias)
-    live = hidden_in.shape[0]
-    extra = ((0, -live % 16), (0, 0))
-    partial_out = jnp.dot(jnp.pad(attended, extra), w_out, preferred_element_type=jnp.float32)
+    tokens, half = hidden_in.shape
+    padded = tokens + -tokens % 16
+    width = 2 * half
     experts = lax.axis_size("ep")
-    route_weight = route_scores / jnp.sum(route_scores, axis=1, keepdims=True)
-    named = route_ids[:, :, None] == jnp.arange(experts, dtype=jnp.int32)[None, None, :]
-    dense = jnp.sum(jnp.where(named, route_weight[:, :, None], 0.0), axis=1)
-    high = lax.reduce_precision(dense, 8, 7)
-    coded = jnp.concatenate([high, dense - high], axis=1).astype(jnp.bfloat16)
-    coded = jnp.pad(coded, (extra[0], (0, -coded.shape[1] % 128)))
-    hidden_out = expert_layer(
-        partial_out,
-        jnp.pad(gathered, extra),
+    heads = break_bias.shape[0]
+    zs = experts // 4
+    extra = 2 * experts + -2 * experts % 128
+    blocks = (2, zs, 2, padded, half // 2)
+    bf16, f32 = jnp.bfloat16, jnp.float32
+    vmem = pl.BlockSpec(memory_space=pltpu.VMEM)
+    smem = pl.BlockSpec(memory_space=pltpu.SMEM)
+    hbm = pl.BlockSpec(memory_space=pl.ANY)
+    dma = pltpu.SemaphoreType.DMA
+    columns_in, span = key_cache.shape[1:]
+    sizes = (tokens, padded, zs, width, half, experts, heads)
+    new_shape = jax.ShapeDtypeStruct((tokens, columns_in), bf16)
+    pairs = [4, zs - 1, zs, 2 * zs, 4 * zs, 3 + zs, 2 * zs, zs]
+    return pl.pallas_call(
+        functools.partial(layer_kernel, sizes),
+        out_shape=(jax.ShapeDtypeStruct((tokens, half), bf16), new_shape, new_shape),
+        in_specs=[vmem, vmem, smem, smem, vmem, vmem, vmem] + [hbm] * 9,
+        out_specs=(vmem, vmem, vmem),
+        scratch_shapes=[
+            pltpu.VMEM((3,) + w_query.shape, bf16),
+            pltpu.VMEM(key_cache.shape, bf16),
+            pltpu.VMEM(value_cache.shape, bf16),
+            pltpu.VMEM((2,) + w_out.shape, bf16),
+            pltpu.VMEM(expert_gate.shape[1:], bf16),
+            pltpu.VMEM(expert_up.shape[1:], bf16),
+            pltpu.VMEM(expert_down.shape[1:], bf16),
+            pltpu.VMEM((2, tokens, half), bf16),
+            pltpu.VMEM((padded, width), bf16),
+            pltpu.VMEM((heads, padded, span), f32),
+            pltpu.VMEM((padded, span), jnp.int32),
+            pltpu.VMEM((heads, padded, span), f32),
+            pltpu.VMEM((2, padded, columns_in), bf16),
+            pltpu.VMEM((tokens, half), f32),
+            pltpu.VMEM((2, 2, zs, 2, padded, half + extra), bf16),
+            pltpu.VMEM((2,) + blocks, f32),
+            pltpu.VMEM((2,) + blocks, bf16),
+            pltpu.VMEM((2,) + blocks, bf16),
+            pltpu.VMEM(blocks, bf16),
+            pltpu.VMEM(blocks, bf16),
+            pltpu.VMEM(blocks[1:], bf16),
+            pltpu.VMEM(blocks[1:], bf16),
+            pltpu.VMEM(blocks[1:], bf16),
+            pltpu.VMEM((zs - 1,) + blocks[2:], bf16),
+            pltpu.VMEM(blocks[2:], f32),
+            pltpu.VMEM(blocks[3:], f32),
+            dma((9,)),
+        ]
+        + [dma((count,)) for count in pairs for _ in range(2)],
+        compiler_params=pltpu.CompilerParams(
+            collective_id=0, has_side_effects=True, vmem_limit_bytes=60 * 1024 * 1024
+        ),
+    )(
+        hidden_in,
+        attn_gain[None, :],
+        break_bias,
+        lengths,
         ffn_gain[None, :],
-        coded,
+        route_ids,
+        route_scores,
+        w_query,
+        w_key,
+        w_value,
+        key_cache,
+        value_cache,
+        w_out,
         expert_gate,
         expert_up,
         expert_down,
-        live,
-        experts,
-    )
-    return (hidden_out[:live], new_keys, new_values)
+    )
 
 
 def solution(mesh):

time: 74.9 us -> 58.2 us (0.78)
  matrix products: 9.74 us -> 0 us
  blocking collectives: 5.99 us -> 0 us
  other arithmetic: 4.38 us -> 0 us
  local copies, waits for them, and re-layouts: 4.3 us -> 6.73 us
  Pallas kernels: 49 us -> 50.5 us
    dot_general x9 -> x0, matrix products: 9.74 us -> none  [the longest x3 5.25 us: project_rows(): lax.dot_general(normed, weight, (((1,), (1,)), ((), ())), preferred_eleme...]
    all_gather x1 -> x0, blocking collectives: 5.99 us -> none  [dense_shards(): gathered = lax.all_gather(hidden_in, 'tp', axis=1, tiled=True)]
    unnamed x6 -> x5, local copies, waits for them, and re-layouts: 1.75 us -> 6.73 us
    pallas_call x1, Pallas kernels: 49 us -> 50.5 us  [dense_shards(): pl.pallas_call(functools.partial(layer_kernel, sizes), out_shape=(jax.Sha...]
    reduce_sum x3 -> x0, other arithmetic: 1.55 us -> none  [the longest x1 0.71 us: dense_shards(): dense = jnp.sum(jnp.where(named, route_weight[:, :, None], 0.0), axis=1)]
    slice x1 -> x0, local copies, waits for them, and re-layouts: 1.42 us -> none  [dense_shards(): return (hidden_out[:live], new_keys, new_values)]
where the time goes in v2:
time: 58.2 us; the launch traced here: 57.9 us
  Pallas kernels  50.5 us (87%)
  local copies, waits for them, and re-layouts  6.73 us (12%)
  between operations  0.64 us (1%)
    pallas_call x1, Pallas kernels, dense_shards(): pl.pallas_call(functools.partial(layer_kernel, sizes), out_shape=(jax.Sha...  50.5 us
    unnamed x5, local copies, waits for them, and re-layouts  6.73 us

profile of v2, /device:TPU:0, one launch (start us, length us, event | category | flops | bytes accessed | tf_op | source)
XLA Modules:
  0.0 57.9 jit_solution(5170895148834567515)
XLA Ops:
  0.6 1.4 %copy.19.ids_ref = s32[20,6]{1,0:T(8,128)} copy(s32[20,6]{0,1:T(8,128)} %param.27) | data formatting | bytes 960 | tf_op args[11]
  2.0 1.4 %copy.20.scores_ref = f32[20,6]{1,0:T(8,128)} copy(f32[20,6]{0,1:T(8,128)} %param.28) | data formatting | bytes 960 | tf_op args[12]
  3.4 50.5 %shard_map.175 = (bf16[20,1024]{1,0:T(8,128)(2,1)}, bf16[20,128]{1,0:T(8,128)(2,1)}, bf16[20,128]{1,0:T(8,128)(2,1)}) custom-call(bf16[20,1024]{1,0:T(8,128)(2,1)} %hid_ref.1, f32[1,2048]{1,0:T(1,128)} %bitcast.2, f32[2]{0:T(128)} %bias_ref.1, s32[20]{0:T(128)} %lengths_ref.1, f32[1,2048]{1,0:T(1,128)} %bitcast.3, s32[20,6]{1,0:T(8,128)} %copy.19.ids_ref, ...), custom_call_target="tpu_custom_call" | custom-call | tf_op jit(solution)/shard_map/pallas_call | solution.py:546
  53.9 1.4 %copy.24 = bf16[20,1024]{1,0:T(8,128)(2,1)} copy(bf16[20,1024]{1,0:T(8,128)(2,1)} %get-tuple-element.6) | data formatting | bytes 81920
  55.3 1.3 %copy.25 = bf16[20,128]{1,0:T(8,128)(2,1)} copy(bf16[20,128]{1,0:T(8,128)(2,1)} %get-tuple-element.7) | data formatting | bytes 10240
  56.6 1.3 %copy.26 = bf16[20,128]{1,0:T(8,128)(2,1)} copy(bf16[20,128]{1,0:T(8,128)(2,1)} %get-tuple-element.8) | data formatting | bytes 10240

commit v3 on v2

--- a/solution.py
+++ b/solution.py
@@ -132,6 +132,11 @@
     return (hidden_out, new_keys, new_values)
 
 
+def hand_on(*refs):
+    for source, target in zip(refs[:3], refs[3:]):
+        target[...] = source[...]
+
+
 def layer_kernel(
     sizes,
     hid_ref,
@@ -165,6 +170,7 @@
     logits,
     spans,
     stick,
+    turn,
     att_both,
     resid,
     rows,
@@ -230,7 +236,7 @@
     loads = [
         pltpu.make_async_copy(src, dst, load_sem.at[i]) for i, (src, dst) in enumerate(sources)
     ]
-    for load in loads:
+    for load in loads[:6]:
         load.start()
 
     barrier = pltpu.get_barrier_semaphore()
@@ -268,18 +274,20 @@
     normed_in[...] = jnp.zeros_like(normed_in)
 
     scores = scores_ref[...]
-    route_weight = scores / jnp.sum(scores, axis=1, keepdims=True)
+    route_weight = scores / jnp.sum(scores, axis=0, keepdims=True)
     high = route_weight.astype(jnp.bfloat16).astype(jnp.float32)
     low = route_weight - high
     ids = ids_ref[...]
     extra = rows.shape[-1] - half
-    lane = lax.broadcasted_iota(jnp.int32, (tokens, extra), 1)
-    coded = jnp.zeros((tokens, extra), jnp.float32)
-    for k in range(ids.shape[1]):
-        name = ids[:, k : k + 1]
-        coded += jnp.where(lane == name, high[:, k : k + 1], 0.0)
-        coded += jnp.where(lane == name + experts, low[:, k : k + 1], 0.0)
-    rows[y, x, z, c, :tokens, half:] = coded.astype(jnp.bfloat16)
+    place = lax.broadcasted_iota(jnp.int32, (extra, tokens), 0)
+    coded = jnp.zeros((extra, tokens), jnp.float32)
+    for k in range(ids.shape[0]):
+        name = ids[k : k + 1]
+        coded += jnp.where(place == name, high[k : k + 1], 0.0)
+        coded += jnp.where(place == name + experts, low[k : k + 1], 0.0)
+    turn[...] = jnp.zeros_like(turn)
+    turn[:, :tokens] = coded
+    rows[y, x, z, c, :tokens, half:] = turn[...].T[:tokens].astype(jnp.bfloat16)
 
     give.wait_recv()
     left = hid_both[0].astype(jnp.float32)
@@ -306,6 +314,8 @@
     span = key_c.shape[2]
     q_lane = lax.broadcasted_iota(jnp.int32, q_cols.shape, 1)
     loads[3].wait()
+    for load in loads[6:]:
+        load.start()
 
     def score(t, carry):
         column = jnp.sum(jnp.where(q_lane == t, q_cols, 0.0), axis=1, keepdims=True)
@@ -316,7 +326,7 @@
         spans[pl.ds(t, 1), :] = jnp.full((1, span), lengths_ref[t], jnp.int32)
         return carry
 
-    lax.fori_loop(0, tokens, score, 0, unroll=2)
+    lax.fori_loop(0, tokens, score, 0, unroll=5)
     row = lax.broadcasted_iota(jnp.int32, (span, span), 0)
     col = lax.broadcasted_iota(jnp.int32, (span, span), 1)
     later = (row > col).astype(jnp.float32).astype(jnp.bfloat16)
@@ -347,7 +357,7 @@
         return jnp.where(att_lane == t, column, gathered)
 
     gathered = lax.fori_loop(
-        0, tokens, attend, jnp.zeros((columns_in, 128), jnp.float32), unroll=2
+        0, tokens, attend, jnp.zeros((columns_in, 128), jnp.float32), unroll=5
     )
     att_both[y] = gathered.T[:padded].astype(jnp.bfloat16)
     give_att = send(
@@ -543,7 +553,7 @@
     sizes = (tokens, padded, zs, width, half, experts, heads)
     new_shape = jax.ShapeDtypeStruct((tokens, columns_in), bf16)
     pairs = [4, zs - 1, zs, 2 * zs, 4 * zs, 3 + zs, 2 * zs, zs]
-    return pl.pallas_call(
+    results = pl.pallas_call(
         functools.partial(layer_kernel, sizes),
         out_shape=(jax.ShapeDtypeStruct((tokens, half), bf16), new_shape, new_shape),
         in_specs=[vmem, vmem, smem, smem, vmem, vmem, vmem] + [hbm] * 9,
@@ -561,6 +571,7 @@
             pltpu.VMEM((heads, padded, span), f32),
             pltpu.VMEM((padded, span), jnp.int32),
             pltpu.VMEM((heads, padded, span), f32),
+            pltpu.VMEM((extra, 128), f32),
             pltpu.VMEM((2, padded, columns_in), bf16),
             pltpu.VMEM((tokens, half), f32),
             pltpu.VMEM((2, 2, zs, 2, padded, half + extra), bf16),
@@ -587,8 +598,8 @@
         break_bias,
         lengths,
         ffn_gain[None, :],
-        route_ids,
-        route_scores,
+        route_ids.T,
+        route_scores.T,
         w_query,
         w_key,
         w_value,
@@ -599,6 +610,12 @@
         expert_up,
         expert_down,
     )
+    return pl.pallas_call(
+        hand_on,
+        out_shape=tuple(jax.ShapeDtypeStruct(r.shape, r.dtype) for r in results),
+        in_specs=[vmem] * 3,
+        out_specs=(vmem, vmem, vmem),
+    )(*results)
 
 
 def solution(mesh):

time: 58.2 us -> 52.5 us (0.902)
  local copies, waits for them, and re-layouts: 6.73 us -> 0 us
  Pallas kernels: 50.5 us -> 51.6 us
    unnamed x5 -> x0, local copies, waits for them, and re-layouts: 6.73 us -> none
    pallas_call x0 -> x1, Pallas kernels: none -> 1.45 us  [dense_shards(): pl.pallas_call(hand_on, out_shape=tuple((jax.ShapeDtypeStruct(r.shape, r....]
where the time goes in v3:
time: 52.5 us; the launch traced here: 52.3 us
  Pallas kernels  51.6 us (98%)
  between operations  0.65 us (1%)
    pallas_call x1, Pallas kernels, dense_shards(): pl.pallas_call(functools.partial(layer_kernel, sizes), out_shape=(jax.Sha...  50.2 us
    pallas_call x1, Pallas kernels, dense_shards(): pl.pallas_call(hand_on, out_shape=tuple((jax.ShapeDtypeStruct(r.shape, r....  1.45 us

profile of v3, /device:TPU:0, one launch (start us, length us, event | category | flops | bytes accessed | tf_op | source)
XLA Modules:
  0.0 52.3 jit_solution(6560378433947367639)
XLA Ops:
  0.6 50.2 %shard_map.175 = (bf16[20,1024]{1,0:T(8,128)(2,1)}, bf16[20,128]{1,0:T(8,128)(2,1)}, bf16[20,128]{1,0:T(8,128)(2,1)}) custom-call(bf16[20,1024]{1,0:T(8,128)(2,1)} %hid_ref.1, f32[1,2048]{1,0:T(1,128)} %bitcast.4, f32[2]{0:T(128)} %bias_ref.1, s32[20]{0:T(128)} %lengths_ref.1, f32[1,2048]{1,0:T(1,128)} %bitcast.5, s32[6,20]{1,0:T(8,128)} %bitcast.6, ...), custom_call_target="tpu_custom_call" | custom-call | tf_op jit(solution)/shard_map/pallas_call | solution.py:556
  50.8 1.4 %shard_map.176 = (bf16[20,1024]{1,0:T(8,128)(2,1)}, bf16[20,128]{1,0:T(8,128)(2,1)}, bf16[20,128]{1,0:T(8,128)(2,1)}) custom-call(bf16[20,1024]{1,0:T(8,128)(2,1)} %get-tuple-element.6.refs_0_, bf16[20,128]{1,0:T(8,128)(2,1)} %get-tuple-element.7.refs_1_, bf16[20,128]{1,0:T(8,128)(2,1)} %get-tuple-element.8.refs_2_), custom_call_target="tpu_custom_call" | custom-call | tf_op jit(solution)/shard_map/pallas_call | solution.py:613
